TPU v7x, 32 devices: a whole 2x2x4 slice. The times are simulated.
32 devices in a mesh: dp: 2 (over y), kv: 16 (over z, x, core), tp: 1.
Axes of the slice: x: 2, y: 2, z: 4, core: 2. Of those that a mesh axis runs over, the one named last changes fastest.
Arguments:
- tokens: bfloat16 [16, 4096], P('dp', 'kv'), may hold values from -6 to 6
- attn_gain: float32 [4096], P('kv'), may hold values from 0.1 to 1.9
- query_weight: bfloat16 [4096, 2048], P('kv', 'tp'), may hold values from -0.09375 to 0.09375
- key_cache: bfloat16 [16, 2048, 8, 2, 128], P('dp', 'kv', 'tp'), may hold values from -1024 to 1024
- value_cache: bfloat16 [16, 2048, 8, 256], P('dp', 'kv', 'tp'), may hold values from -6 to 6
- lambdas: float32 [8], P('tp'), may hold values from 0.3 to 0.8
- head_gain: float32 [256], replicated, may hold values from 0.1 to 1.9
- out_weight: bfloat16 [2048, 4096], P('tp', 'kv'), may hold values from -0.125 to 0.125
- mixer_gain: float32 [4096], P('kv'), may hold values from 0.1 to 1.9
- up_weight: bfloat16 [4096, 16384], P('kv', 'tp'), may hold values from -0.09375 to 0.09375
- down_weight: bfloat16 [16384, 4096], P('tp', 'kv'), may hold values from -0.046875 to 0.046875
Outputs:
- result: bfloat16 [16, 4096], P('dp', 'kv')
All inputs are finite; a program needn't handle non-finite values.
Results may differ from a plain program's by a relative error of at most 0.024.
Values may be sent and summed in bfloat16 or wider, within the bound.
A program may use at most 64 MiB of HBM per device.

v0:
```python
import math

import jax
import jax.numpy as jnp
from jax import lax
from jax.sharding import PartitionSpec as P

D = 4096


EPS = 1e-05


def merged(value, axis, combine):
    everything = jax.tree.map(lambda part: lax.all_gather(part, axis), value)
    initial = jax.tree.map(lambda part: part[0], everything)

    def lap(k, so_far):
        return combine(so_far, jax.tree.map(lambda part: part[k], everything))

    return lax.fori_loop(1, lax.axis_size(axis), lap, initial)


def rotate(query, position):
    half = query.shape[-1] // 2
    inverse = 10000.0 ** (-jnp.arange(half, dtype=jnp.float32) / half)
    angle = jnp.float32(position) * inverse
    cosine = jnp.cos(angle)
    sine = jnp.sin(angle)
    first = query[..., :half]
    second = query[..., half:]
    return jnp.concatenate(
        [first * cosine - second * sine, second * cosine + first * sine], axis=-1
    )


def combine_partial(earlier, later):
    top_a, total_a, numer_a = earlier
    top_b, total_b, numer_b = later
    top = jnp.maximum(top_a, top_b)
    factor_a = jnp.exp(top_a - top)
    factor_b = jnp.exp(top_b - top)
    return (
        top,
        total_a * factor_a + total_b * factor_b,
        numer_a * factor_a[..., None] + numer_b * factor_b[..., None],
    )


def local(
    tokens,
    attn_gain,
    query_weight,
    key_cache,
    value_cache,
    lambdas,
    head_gain,
    out_weight,
    mixer_gain,
    up_weight,
    down_weight,
):
    row_count = tokens.shape[0]
    local_heads = key_cache.shape[2]
    head_width = key_cache.shape[4]
    length = key_cache.shape[1] * lax.axis_size("kv")
    tok_float = tokens.astype(jnp.float32)
    own_squares = jnp.sum(tok_float * tok_float, axis=1)
    scaled_in = (tok_float * attn_gain).astype(jnp.bfloat16)
    query_part = jnp.dot(scaled_in, query_weight, preferred_element_type=jnp.float32)
    squares = lax.psum(own_squares, "kv")
    query_raw = lax.psum(query_part, "kv")
    attn_inv = lax.rsqrt(squares / D + EPS)
    shaped = (attn_inv[:, None] * query_raw).reshape(row_count, local_heads, 2, head_width)
    query = rotate(shaped, length - 1).astype(jnp.bfloat16)
    scores = jnp.einsum(
        "bhcd,bkhcd->bhck", query, key_cache, preferred_element_type=jnp.float32
    ) / math.sqrt(head_width)
    top = jnp.max(scores, axis=-1)
    expo = jnp.exp(scores - top[..., None])
    denom = jnp.sum(expo, axis=-1)
    numer = jnp.einsum(
        "bhck,bkhv->bhcv",
        expo.astype(jnp.bfloat16),
        value_cache,
        preferred_element_type=jnp.float32,
    )
    top, denom, numer = merged((top, denom, numer), "kv", combine_partial)
    ratio = numer / denom[..., None]
    mixed = ratio[:, :, 0] - lambdas[None, :, None] * ratio[:, :, 1]
    normed = mixed * lax.rsqrt(jnp.mean(mixed * mixed, axis=-1, keepdims=True) + EPS) * head_gain
    normed = normed.astype(jnp.bfloat16).reshape(row_count, -1)
    attn_part = jnp.dot(normed, out_weight, preferred_element_type=jnp.float32)
    attn_out = lax.psum(attn_part, "tp")
    middle = (tok_float + attn_out).astype(jnp.bfloat16)
    mid_float = middle.astype(jnp.float32)
    mix_squares = lax.psum(jnp.sum(mid_float * mid_float, axis=1), "kv")
    mixer_inv = lax.rsqrt(mix_squares / D + EPS)
    mixer_in = (mid_float * mixer_gain).astype(jnp.bfloat16)
    up_part = jnp.dot(mixer_in, up_weight, preferred_element_type=jnp.float32)
    share = lax.psum_scatter(up_part, "kv", scatter_dimension=1, tiled=True)
    hidden_share = jnp.square(jax.nn.relu(mixer_inv[:, None] * share)).astype(jnp.bfloat16)
    mixer_part = jnp.dot(
        lax.all_gather(hidden_share, "kv", axis=1, tiled=True),
        down_weight,
        preferred_element_type=jnp.float32,
    )
    mixer_out = lax.psum(mixer_part, "tp")
    return (mid_float + mixer_out).astype(jnp.bfloat16)


def solution(mesh):
    return jax.shard_map(
        local,
        mesh=mesh,
        in_specs=(
            P("dp", "kv"),
            P("kv"),
            P("kv", "tp"),
            P("dp", "kv", "tp", None, None),
            P("dp", "kv", "tp", None),
            P("tp"),
            P(),
            P("tp", "kv"),
            P("kv"),
            P("kv", "tp"),
            P("tp", "kv"),
        ),
        out_specs=P("dp", "kv"),
        check_vma=False,
    )
```

profile of v0, /device:TPU:0, one launch (start us, length us, event | category | flops | bytes accessed | tf_op | source)
XLA Modules:
  0.0 270.8 jit_solution(3176983266643035362)
XLA Ops:
  6.5 0.9 fusion.19
  7.4 0.3 copy-done
  7.8 1.6 fusion.22
  9.4 34.9 %psum.20 = f32[8]{0:T(128)S(1)} all-reduce(f32[8]{0:T(128)S(1)} %fusion.19), channel_id=1, replica_groups=mesh['dp'=2,'kv'=16,'tp'=1] {'kv'}, use_global_device_ids=true, to_apply=%region_1.0 | all-reduce | flops 8 | bytes 64 | tf_op jit(solution)/shard_map/psum | solution.py:71
  44.4 55.3 %all-reduce.2.cloned.1.call-done = f32[8,2048]{1,0:T(8,128)} async-done(((f32[8,2048]{1,0:T(8,128)}), f32[8,2048]{1,0:T(8,128)}) %all-reduce.2.cloned.1.call-update) | async-done | bytes 65552 | tf_op jit(solution)/shard_map/psum | solution.py:72
  99.7 1.1 broadcast_multiply_fusion
  101.0 4.5 %fusion.5 = f32[8,8,2,1,128]{4,3,2,1,0:T(1,128)S(1)} fusion(bf16[8,128,8,2,128]{4,3,2,1,0:T(2,128)(2,1)} %param.16, bf16[8,8,2,128,1]{3,0,2,1,4:T(8,128)(2,1)S(1)} %maximum_bitcast_fusion), kind=kOutput, calls=%fused_computation.13 | convolution fusion | flops 4194304 | bytes 4292608 | tf_op jit(solution)/shard_map/bhcd,bkhcd->bhck/dot_general | solution.py:76
  105.5 0.2 multiply_reduce_fusion
  105.6 0.8 fusion.7
  106.5 0.7 copy.48
  107.4 22.6 %all-gather = f32[128,8,2]{1,2,0:T(2,128)S(1)} all-gather(f32[8,8,2]{1,2,0:T(2,128)S(1)} %copy.45), channel_id=2, replica_groups=mesh['dp'=2,'kv'=16,'tp'=1] {'kv'}, dimensions={0}, use_global_device_ids=true | all-gather | bytes 8704 | tf_op jit(solution)/shard_map/all_gather | solution.py:15
  130.0 0.3 fusion.26
  130.4 18.1 %all-gather.1 = f32[128,8,2]{1,2,0:T(2,128)S(1)} all-gather(f32[8,8,2]{1,2,0:T(2,128)S(1)} %copy.46), channel_id=3, replica_groups=mesh['dp'=2,'kv'=16,'tp'=1] {'kv'}, dimensions={0}, use_global_device_ids=true | all-gather | bytes 8704 | tf_op jit(solution)/shard_map/all_gather | solution.py:15
  148.5 1.9 all-gather.5.cloned.1.call-done
  150.4 0.9 slice.35
  151.4 24.7 %while.19 = (s32[]{:T(128)}, f32[8,8,2]{1,0,2:T(8,128)S(1)}, f32[8,8,2]{1,0,2:T(8,128)S(1)}, f32[8,8,2,256]{3,2,1,0:T(2,128)S(1)}, f32[16,8,8,2]{2,3,1,0:T(2,128...) while((s32[]{:T(128)}, f32[8,8,2]{1,0,2:T(8,128)S(1)}, ...), condition=%wide.region_6.0_spmd, body=%wide.region_5.0_spmd.sunk | while | flops 99077 | bytes 664727 | solution.py:21
  151.5 0.9 constant_dynamic-slice_fusion.6
  152.4 0.1 copy.109
  152.6 0.4 fusion.39
  153.1 0.9 constant_dynamic-slice_fusion.6
  154.0 0.1 copy.109
  154.3 0.4 fusion.39
  154.8 0.9 constant_dynamic-slice_fusion.6
  155.7 0.1 copy.109
  155.9 0.4 fusion.39
  156.4 0.9 constant_dynamic-slice_fusion.6
  157.3 0.1 copy.109
  157.6 0.4 fusion.39
  158.1 0.9 constant_dynamic-slice_fusion.6
  159.0 0.1 copy.109
  159.2 0.4 fusion.39
  159.7 0.9 constant_dynamic-slice_fusion.6
  160.6 0.1 copy.109
  160.9 0.4 fusion.39
  161.4 0.9 constant_dynamic-slice_fusion.6
  162.5 0.4 fusion.39
  163.0 0.9 constant_dynamic-slice_fusion.6
  164.2 0.4 fusion.39
  164.6 0.9 constant_dynamic-slice_fusion.6
  165.8 0.4 fusion.39
  166.3 0.9 constant_dynamic-slice_fusion.6
  167.5 0.4 fusion.39
  167.9 0.9 constant_dynamic-slice_fusion.6
  169.1 0.4 fusion.39
  169.6 0.9 constant_dynamic-slice_fusion.6
  170.5 0.1 copy.109
  170.8 0.4 fusion.39
  171.2 0.9 constant_dynamic-slice_fusion.6
  172.4 0.4 fusion.39
  172.9 0.9 constant_dynamic-slice_fusion.6
  173.8 0.1 copy.109
  174.0 0.4 fusion.39
  174.5 0.9 constant_dynamic-slice_fusion.6
  175.7 0.4 fusion.39
  176.2 0.1 broadcast_divide_fusion
  176.4 0.2 slice_reduce_fusion
  176.6 0.2 fusion.14
  177.0 0.4 multiply_reduce_fusion.1
  177.4 5.4 %fusion.21 = f32[8,16384]{1,0:T(8,128)} fusion(bf16[256,16384]{1,0:T(8,128)(2,1)} %param.22, f32[8,256]{1,0:T(8,128)S(1)} %get-tuple-element.231, f32[256]{0:T(256)S(1)} %copy-done.4), kind=kOutput, calls=%fused_computation.46 | convolution fusion | flops 67112960 | bytes 8922112 | tf_op jit(solution)/shard_map/dot_general | solution.py:100
  182.8 31.6 %psum.24 = f32[8]{0:T(128)S(1)} all-reduce(f32[8]{0:T(128)S(1)} %get-tuple-element.230), channel_id=1, replica_groups=mesh['dp'=2,'kv'=16,'tp'=1] {'kv'}, use_global_device_ids=true, to_apply=%region_9.0 | all-reduce | flops 8 | bytes 64 | tf_op jit(solution)/shard_map/psum | solution.py:97
  214.4 23.7 %reduce-scatter.2.cloned.1.call-done = f32[8,1024]{1,0:T(8,128)} async-done(((f32[8,16384]{1,0:T(8,128)}), f32[8,1024]{1,0:T(8,128)}) %reduce-scatter.2.cloned.1.call-update) | async-done | bytes 32784 | tf_op jit(solution)/shard_map/reduce_scatter | solution.py:101
  238.2 0.8 multiply_convert_fusion.2
  239.0 20.1 %all_gather.27 = bf16[8,16384]{1,0:T(8,128)(2,1)S(1)} all-gather(bf16[8,1024]{1,0:T(8,128)(2,1)S(1)} %multiply_convert_fusion.2), channel_id=1, replica_groups=mesh['dp'=2,'kv'=16,'tp'=1] {'kv'}, dimensions={1}, use_global_device_ids=true | all-gather | bytes 278528 | tf_op jit(solution)/shard_map/all_gather | solution.py:104
  259.1 5.2 %fusion.11 = bf16[8,256]{1,0:T(8,128)(2,1)} fusion(f32[8,256]{1,0:T(8,128)S(1)} %get-tuple-element.231, bf16[8,16384]{1,0:T(8,128)(2,1)S(1)} %all_gather.27, bf16[16384,256]{1,0:T(8,128)(2,1)} %param.23), kind=kOutput, calls=%fused_computation.21 | convolution fusion | flops 67112960 | bytes 8663040 | tf_op jit(solution)/shard_map/dot_general | solution.py:103
  (94 shorter events, 4.2 us)
Async XLA Ops:
  6.5 1.2 copy-start
  6.5 93.2 %all-reduce.2.cloned.1.call-start = ((), (), s32[]{:S(2)}) async-start(), calls=%async_computation.1 | async-start | bytes 131072 | tf_op jit(solution)/shard_map/psum | solution.py:72
  9.4 141.1 %all-gather.5.cloned.1.call-start = ((), (), s32[]{:S(2)}) async-start(), calls=%async_computation.3 | async-start | bytes 2228224 | tf_op jit(solution)/shard_map/all_gather | solution.py:15
  99.7 5.9 %copy-start.1 = (bf16[8,128,8,256]{3,2,1,0:T(8,128)(2,1)S(1)}, bf16[8,128,8,256]{3,2,1,0:T(8,128)(2,1)}, u32[]{:S(2)}) copy-start(bf16[8,128,8,256]{3,2,1,0:T(8,128)(2,1)} %param.17) | copy-start | bytes 12582916
  100.9 6.2 %copy-start.6 = (f32[256]{0:T(256)S(1)}, f32[256]{0:T(256)}, u32[]{:S(2)}) copy-start(f32[256]{0:T(256)} %param.19) | copy-start | bytes 3076
  101.0 6.3 %copy-start.5 = (f32[8]{0:T(128)S(1)}, f32[8]{0:T(128)}, u32[]{:S(2)}) copy-start(f32[8]{0:T(128)} %param.18) | copy-start | bytes 100
  106.5 70.6 %copy-start.2 = (bf16[2048,256]{1,0:T(8,128)(2,1)S(1)}, bf16[2048,256]{1,0:T(8,128)(2,1)}, u32[]{:S(2)}) copy-start(bf16[2048,256]{1,0:T(8,128)(2,1)} %param.20) | copy-start | bytes 3145732
  106.5 70.6 %copy-start.3 = (bf16[8,256]{1,0:T(8,128)(2,1)S(1)}, bf16[8,256]{1,0:T(8,128)(2,1)}, u32[]{:S(2)}) copy-start(bf16[8,256]{1,0:T(8,128)(2,1)} %param.13) | copy-start | bytes 12292
  107.1 131.0 %reduce-scatter.2.cloned.1.call-start = ((), (), s32[]{:S(2)}) async-start(), calls=%async_computation.2 | async-start | bytes 557056 | tf_op jit(solution)/shard_map/reduce_scatter | solution.py:101
  107.4 70.0 %copy-start.4 = (f32[256]{0:T(256)S(1)}, f32[256]{0:T(256)}, u32[]{:S(2)}) copy-start(f32[256]{0:T(256)} %param.21) | copy-start | bytes 3076
Sparse Core Ops, SparseCore 0:
  10.8 88.8 all-reduce.1
  107.3 43.1 all-gather.4
  182.9 55.1 reduce-scatter.1
where the time goes:
time: 271 us
  blocking collectives  127 us (47%)
  waiting for transfers between devices  81 us (30%)
  local copies, waits for them, and re-layouts  20.5 us (8%)
  matrix products  17.8 us (7%)
  between operations  13.3 us (5%)
  other arithmetic  10.3 us (4%)
    psum x1, waiting for transfers between devices, local(): query_raw = lax.psum(query_part, 'kv')  55.3 us
    all_gather x2, blocking collectives, merged(): everything = jax.tree.map(lambda part: lax.all_gather(part, axis), value)  40.7 us
    psum x1, blocking collectives, local(): squares = lax.psum(own_squares, 'kv')  34.9 us
    psum x1, blocking collectives, local(): mix_squares = lax.psum(jnp.sum(mid_float * mid_float, axis=1), 'kv')  31.6 us
    reduce_scatter x1, waiting for transfers between devices, local(): share = lax.psum_scatter(up_part, 'kv', scatter_dimension=1, tiled=True)  23.7 us
    all_gather x1, blocking collectives, local(): lax.all_gather(hidden_share, 'kv', axis=1, tiled=True)  20.1 us
    dynamic_slice x30, local copies, waits for them, and re-layouts, lap(): return combine(so_far, jax.tree.map(lambda part: part[k], everything))  13.9 us
    add x15, other arithmetic, combine_partial(): numer_a * factor_a[..., None] + numer_b * factor_b[..., None]  6.36 us
  transfers between devices with their start and end apart: 3, of which 3 were waited for; matrix products, arithmetic and copies ran while one was open for 0% of the time, Pallas kernels for 0%

commit v1 on v0

--- a/solution.py
+++ b/solution.py
@@ -1,14 +1,17 @@
+import functools
 import math
 
 import jax
 import jax.numpy as jnp
+import numpy as np
 from jax import lax
+from jax.experimental import pallas as pl
+from jax.experimental.pallas import tpu as pltpu
 from jax.sharding import PartitionSpec as P
 
-D = 4096
-
-
 EPS = 1e-05
+F32 = jnp.float32
+BF16 = jnp.bfloat16
 
 
 def merged(value, axis, combine):
@@ -61,6 +64,7 @@
     down_weight,
 ):
     row_count = tokens.shape[0]
+    width = tokens.shape[1] * lax.axis_size("kv")
     local_heads = key_cache.shape[2]
     head_width = key_cache.shape[4]
     length = key_cache.shape[1] * lax.axis_size("kv")
@@ -70,7 +74,7 @@
     query_part = jnp.dot(scaled_in, query_weight, preferred_element_type=jnp.float32)
     squares = lax.psum(own_squares, "kv")
     query_raw = lax.psum(query_part, "kv")
-    attn_inv = lax.rsqrt(squares / D + EPS)
+    attn_inv = lax.rsqrt(squares / width + EPS)
     shaped = (attn_inv[:, None] * query_raw).reshape(row_count, local_heads, 2, head_width)
     query = rotate(shaped, length - 1).astype(jnp.bfloat16)
     scores = jnp.einsum(
@@ -95,7 +99,7 @@
     middle = (tok_float + attn_out).astype(jnp.bfloat16)
     mid_float = middle.astype(jnp.float32)
     mix_squares = lax.psum(jnp.sum(mid_float * mid_float, axis=1), "kv")
-    mixer_inv = lax.rsqrt(mix_squares / D + EPS)
+    mixer_inv = lax.rsqrt(mix_squares / width + EPS)
     mixer_in = (mid_float * mixer_gain).astype(jnp.bfloat16)
     up_part = jnp.dot(mixer_in, up_weight, preferred_element_type=jnp.float32)
     share = lax.psum_scatter(up_part, "kv", scatter_dimension=1, tiled=True)
@@ -109,9 +113,374 @@
     return (mid_float + mixer_out).astype(jnp.bfloat16)
 
 
+def layer_kernel(
+    n,
+    width,
+    tok_ref,
+    again_ref,
+    lam_ref,
+    hgain_ref,
+    mgain_ref,
+    cos_ref,
+    sin_ref,
+    wq_hbm,
+    k_hbm,
+    v_hbm,
+    wo_hbm,
+    wu_hbm,
+    wd_hbm,
+    out_ref,
+    wq,
+    kc,
+    vc,
+    wo,
+    wu,
+    wd,
+    q_send,
+    q_recv,
+    q_all,
+    a_send,
+    a_recv,
+    n_all,
+    u_send,
+    u_recv,
+    h_all,
+    load_sem,
+    send_sem,
+    recv_sem,
+):
+    rows, feats = tok_ref.shape
+    hd = cos_ref.shape[1]
+    maps = wq.shape[1] // hd
+    heads = maps // 2
+    vdim = vc.shape[2]
+    share = wu.shape[1] // n
+    per = maps * rows // n
+    me = lax.axis_index("kv")
+
+    loads = [
+        pltpu.make_async_copy(src, dst, load_sem.at[i])
+        for i, (src, dst) in enumerate(
+            [(wq_hbm, wq), (k_hbm, kc), (v_hbm, vc), (wo_hbm, wo), (wu_hbm, wu), (wd_hbm, wd)]
+        )
+    ]
+    loads[0].start()
+    loads[1].start()
+
+    barrier = pltpu.get_barrier_semaphore()
+
+    def greet(k, carry):
+        pl.semaphore_signal(barrier, inc=1, device_id={"kv": lax.rem(me + k, n)})
+        return carry
+
+    lax.fori_loop(1, n, greet, 0)
+
+    def to_peer(phase, k, src, dst):
+        return pltpu.make_async_remote_copy(
+            src_ref=src,
+            dst_ref=dst,
+            send_sem=send_sem.at[phase, k],
+            recv_sem=recv_sem.at[phase, k],
+            device_id={"kv": lax.rem(me + k, n)},
+        )
+
+    def over_peers(body):
+        lax.fori_loop(1, n, lambda k, c: (body(k), c)[1], 0)
+
+    tok = tok_ref[...].astype(F32)
+    squares = jnp.sum(tok * tok, axis=1, keepdims=True)
+    scaled = (tok * again_ref[...]).astype(BF16)
+    loads[0].wait()
+    for load in loads[2:]:
+        load.start()
+    query = jnp.dot(scaled, wq[...], preferred_element_type=F32)
+    for m in range(n):
+        q_send[m, :, :hd] = query[:, m * hd : (m + 1) * hd]
+        q_send[m, :, hd:] = jnp.broadcast_to(squares, (rows, hd))
+    pl.semaphore_wait(barrier, n - 1)
+    over_peers(
+        lambda k: to_peer(0, k, q_send.at[lax.rem(me + k, n)], q_recv.at[k]).start()
+    )
+    total = q_send[me]
+    for k in range(1, n):
+        to_peer(0, k, q_send.at[0], q_recv.at[k]).wait_recv()
+        total += q_recv[k]
+    inv = lax.rsqrt(total[:, hd:] / width + EPS)
+    raw = inv * total[:, :hd]
+    turned = raw * cos_ref[...] + pltpu.roll(raw, hd // 2, 1) * sin_ref[...]
+    q_all[me] = turned.astype(BF16)
+    over_peers(lambda k: to_peer(1, k, q_all.at[me], q_all.at[me]).start())
+    over_peers(
+        lambda k: to_peer(
+            1, k, q_all.at[me], q_all.at[lax.rem(me + n - k, n)]
+        ).wait_recv()
+    )
+
+    q_float = q_all[...].astype(F32)
+    q_rows = jnp.swapaxes(q_float, 0, 1)
+    loads[1].wait()
+    loads[2].wait()
+    lanes = kc.shape[1]
+    own_map = lax.broadcasted_iota(jnp.int32, (maps, lanes), 0) == (
+        lax.broadcasted_iota(jnp.int32, (maps, lanes), 1) % maps
+    )
+    fold = (
+        lax.broadcasted_iota(jnp.int32, (256, 128), 0) // 2
+        == lax.broadcasted_iota(jnp.int32, (256, 128), 1)
+    ).astype(F32).astype(BF16)
+    lane = lax.broadcasted_iota(jnp.int32, (maps, 128), 1)
+    for b in range(rows):
+        scores = lax.dot_general(
+            q_rows[b].astype(BF16),
+            kc[b],
+            (((1,), (1,)), ((), ())),
+            preferred_element_type=F32,
+        ) * (1.0 / math.sqrt(hd))
+        scores = jnp.where(own_map, scores, -jnp.inf)
+        top = jnp.max(scores, axis=1, keepdims=True)
+        expo = jnp.exp(scores - top)
+        denom = jnp.sum(expo, axis=1, keepdims=True)
+        expo_b = expo.astype(BF16)
+        folded = jnp.concatenate(
+            [
+                jnp.dot(expo_b[:, i : i + 256], fold, preferred_element_type=F32)
+                for i in range(0, lanes, 256)
+            ],
+            axis=1,
+        ).astype(BF16)
+        numer = jnp.dot(folded, vc[b], preferred_element_type=F32)
+        stats = jnp.where(lane < 64, top, denom)
+        step = maps // per
+        for part in range(step):
+            slot = b * step + part
+            a_send[slot, :, :vdim] = numer[part * per : (part + 1) * per]
+            a_send[slot, :, vdim:] = stats[part * per : (part + 1) * per]
+    over_peers(
+        lambda k: to_peer(2, k, a_send.at[lax.rem(me + k, n)], a_recv.at[k]).start()
+    )
+    a_recv[0] = a_send[me]
+    for k in range(1, n):
+        to_peer(2, k, a_send.at[0], a_recv.at[k]).wait_recv()
+    tops = [a_recv[k, :, vdim : vdim + 1] for k in range(n)]
+    top = functools.reduce(jnp.maximum, tops)
+    numer = jnp.zeros((per, vdim), F32)
+    denom = jnp.zeros((per, 1), F32)
+    for k in range(n):
+        factor = jnp.exp(tops[k] - top)
+        numer += factor * a_recv[k, :, :vdim]
+        denom += factor * a_recv[k, :, vdim + 64 : vdim + 65]
+    ratio = numer / denom
+    row = lax.broadcasted_iota(jnp.int32, (per, 1), 0)
+    first_head = lax.rem(me, maps // per) * (per // 2)
+    sign = jnp.ones((per, 1), F32)
+    for h in range(per // 2):
+        sign = jnp.where(row == 2 * h + 1, -lam_ref[first_head + h], sign)
+    signed = ratio * sign
+    mixed = signed + pltpu.roll(signed, per - 1, 0)
+    normed = (
+        mixed
+        * lax.rsqrt(jnp.sum(mixed * mixed, axis=1, keepdims=True) / vdim + EPS)
+        * hgain_ref[...]
+    )
+    n_all[me] = normed.astype(BF16)
+    over_peers(lambda k: to_peer(3, k, n_all.at[me], n_all.at[me]).start())
+    over_peers(
+        lambda k: to_peer(
+            3, k, n_all.at[me], n_all.at[lax.rem(me + n - k, n)]
+        ).wait_recv()
+    )
+
+    stacked = n_all[...].astype(F32).reshape(rows * maps, vdim)
+    which = lax.broadcasted_iota(jnp.int32, (rows * maps, vdim), 0) % maps
+    loads[3].wait()
+    spread = jnp.zeros((rows * maps, feats), F32)
+    for h in range(heads):
+        spread += jnp.dot(
+            jnp.where(which == 2 * h, stacked, 0.0).astype(BF16),
+            wo[h * vdim : (h + 1) * vdim, :],
+            preferred_element_type=F32,
+        )
+    attn_out = jnp.sum(spread.reshape(rows, maps, feats), axis=1)
+    middle = (tok_ref[...].astype(F32) + attn_out).astype(BF16).astype(F32)
+    mid_squares = jnp.sum(middle * middle, axis=1, keepdims=True)
+    coarse = mid_squares.astype(BF16).astype(F32)
+    fine = mid_squares - coarse
+    lane8 = lax.broadcasted_iota(jnp.int32, (rows, 128), 1)
+    tail = jnp.where(lane8 < 64, coarse, fine).astype(BF16)
+    mixer_in = (middle * mgain_ref[...]).astype(BF16)
+
+    loads[4].wait()
+
+    def up_share(k):
+        dst = lax.rem(me + k, n)
+        part = jnp.dot(
+            mixer_in,
+            wu[:, pl.ds(pl.multiple_of(dst * share, share), share)],
+            preferred_element_type=F32,
+        )
+        return part
+
+    def up_step(k):
+        u_send[k, :, :share] = up_share(k).astype(BF16)
+        u_send[k, :, share:] = tail
+        to_peer(4, k, u_send.at[k], u_recv.at[k]).start()
+
+    over_peers(up_step)
+    up = up_share(0)
+    mixer_squares = mid_squares
+    for k in range(1, n):
+        to_peer(4, k, u_send.at[k], u_recv.at[k]).wait_recv()
+        up += u_recv[k, :, :share].astype(F32)
+        ends = u_recv[k, :, share:].astype(F32)
+        mixer_squares += ends[:, 0:1] + ends[:, 64:65]
+    mixer_inv = lax.rsqrt(mixer_squares / width + EPS)
+    lifted = jnp.maximum(mixer_inv * up, 0.0)
+    h_all[me] = (lifted * lifted).astype(BF16)
+    over_peers(lambda k: to_peer(5, k, h_all.at[me], h_all.at[me]).start())
+
+    loads[5].wait()
+
+    def down_part(src):
+        return jnp.dot(
+            h_all[src],
+            wd[pl.ds(pl.multiple_of(src * share, share), share), :],
+            preferred_element_type=F32,
+        )
+
+    def down_step(k, so_far):
+        src = lax.rem(me + n - k, n)
+        to_peer(5, k, h_all.at[me], h_all.at[src]).wait_recv()
+        return so_far + down_part(src)
+
+    mixer_out = lax.fori_loop(1, n, down_step, down_part(me))
+    out_ref[...] = (middle + mixer_out).astype(BF16)
+
+    def drain(k):
+        to_peer(0, k, q_send.at[lax.rem(me + k, n)], q_recv.at[k]).wait_send()
+        to_peer(1, k, q_all.at[me], q_all.at[me]).wait_send()
+        to_peer(2, k, a_send.at[lax.rem(me + k, n)], a_recv.at[k]).wait_send()
+        to_peer(3, k, n_all.at[me], n_all.at[me]).wait_send()
+        to_peer(4, k, u_send.at[k], u_recv.at[k]).wait_send()
+        to_peer(5, k, h_all.at[me], h_all.at[me]).wait_send()
+
+    over_peers(drain)
+
+
+def fused(
+    n,
+    tokens,
+    attn_gain,
+    query_weight,
+    key_cache,
+    value_cache,
+    lambdas,
+    head_gain,
+    out_weight,
+    mixer_gain,
+    up_weight,
+    down_weight,
+):
+    rows, feats = tokens.shape
+    _, places, heads, two, hd = key_cache.shape
+    vdim = value_cache.shape[3]
+    maps = heads * two
+    share = up_weight.shape[1] // n
+    per = maps * rows // n
+    half = hd // 2
+    inverse = np.float32(10000.0) ** (-np.arange(half, dtype=np.float32) / np.float32(half))
+    angle = np.float32(places * n - 1) * inverse.astype(np.float32)
+    cosine = np.cos(angle).astype(np.float32)
+    sine = np.sin(angle).astype(np.float32)
+    cos_row = np.concatenate([cosine, cosine])[None]
+    sin_row = np.concatenate([-sine, sine])[None]
+    keys = key_cache.reshape(rows, places * maps, hd)
+    values = value_cache.reshape(rows, places * heads, vdim)
+    vmem = pl.BlockSpec(memory_space=pltpu.VMEM)
+    smem = pl.BlockSpec(memory_space=pltpu.SMEM)
+    hbm = pl.BlockSpec(memory_space=pl.ANY)
+    return pl.pallas_call(
+        functools.partial(layer_kernel, n, feats * n),
+        out_shape=jax.ShapeDtypeStruct((rows, feats), BF16),
+        in_specs=[vmem, vmem, smem] + [vmem] * 4 + [hbm] * 6,
+        out_specs=vmem,
+        scratch_shapes=[
+            pltpu.VMEM(query_weight.shape, BF16),
+            pltpu.VMEM(keys.shape, BF16),
+            pltpu.VMEM(values.shape, BF16),
+            pltpu.VMEM(out_weight.shape, BF16),
+            pltpu.VMEM(up_weight.shape, BF16),
+            pltpu.VMEM(down_weight.shape, BF16),
+            pltpu.VMEM((n, rows, 2 * hd), F32),
+            pltpu.VMEM((n, rows, 2 * hd), F32),
+            pltpu.VMEM((n, rows, hd), BF16),
+            pltpu.VMEM((n, per, vdim + 128), F32),
+            pltpu.VMEM((n, per, vdim + 128), F32),
+            pltpu.VMEM((n, per, vdim), BF16),
+            pltpu.VMEM((n, rows, share + 128), BF16),
+            pltpu.VMEM((n, rows, share + 128), BF16),
+            pltpu.VMEM((n, rows, share), BF16),
+            pltpu.SemaphoreType.DMA((6,)),
+            pltpu.SemaphoreType.DMA((6, n)),
+            pltpu.SemaphoreType.DMA((6, n)),
+        ],
+        compiler_params=pltpu.CompilerParams(
+            collective_id=0, has_side_effects=True, vmem_limit_bytes=60 * 1024 * 1024
+        ),
+    )(
+        tokens,
+        attn_gain[None],
+        lambdas,
+        head_gain[None],
+        mixer_gain[None],
+        jnp.asarray(cos_row),
+        jnp.asarray(sin_row),
+        query_weight,
+        keys,
+        values,
+        out_weight,
+        up_weight,
+        down_weight,
+    )
+
+
+def fits(
+    n,
+    tokens,
+    attn_gain,
+    query_weight,
+    key_cache,
+    value_cache,
+    lambdas,
+    head_gain,
+    out_weight,
+    mixer_gain,
+    up_weight,
+    down_weight,
+):
+    rows, feats = tokens.shape
+    _, places, heads, two, hd = key_cache.shape
+    maps = heads * two
+    return (
+        lax.axis_size("tp") == 1
+        and n == maps
+        and hd == 128
+        and rows % 8 == 0
+        and maps * rows == 8 * n
+        and maps % 8 == 0
+        and feats % 128 == 0
+        and (places * maps) % 256 == 0
+        and up_weight.shape[1] % (128 * n) == 0
+    )
+
+
+def layer(*args):
+    n = lax.axis_size("kv")
+    return fused(n, *args) if fits(n, *args) else local(*args)
+
+
 def solution(mesh):
     return jax.shard_map(
-        local,
+        layer,
         mesh=mesh,
         in_specs=(
             P("dp", "kv"),

time: 271 us -> 52.6 us (0.19)
  blocking collectives: 127 us -> 0 us
  waiting for transfers between devices: 81 us -> 0 us
  Pallas kernels: 0 us -> 51.1 us
  local copies, waits for them, and re-layouts: 20.5 us -> 1.28 us
  matrix products: 17.8 us -> 0 us
  between operations: 13.3 us -> 0.01 us
  other arithmetic: 10.3 us -> 0 us
    psum x2 -> x0, blocking collectives: 66.6 us -> none  [the longest x1 34.9 us: local(): squares = lax.psum(own_squares, 'kv')]
    all_gather x3 -> x0, blocking collectives: 60.8 us -> none  [the longest x2 40.7 us: merged(): everything = jax.tree.map(lambda part: lax.all_gather(part, axis), value)]
    psum x1 -> x0, waiting for transfers between devices: 55.3 us -> none  [local(): query_raw = lax.psum(query_part, 'kv')]
    pallas_call x0 -> x1, Pallas kernels: none -> 51.1 us  [fused(): pl.pallas_call(functools.partial(layer_kernel, n, feats * n), out_shape=j...]
    reduce_scatter x1 -> x0, waiting for transfers between devices: 23.7 us -> none  [local(): share = lax.psum_scatter(up_part, 'kv', scatter_dimension=1, tiled=True)]
    dot_general x6 -> x0, matrix products: 17.8 us -> none  [the longest x1 5.37 us: local(): up_part = jnp.dot(mixer_in, up_weight, preferred_element_type=jnp.float32)]
    dynamic_slice x30 -> x0, local copies, waits for them, and re-layouts: 13.9 us -> none  [lap(): return combine(so_far, jax.tree.map(lambda part: part[k], everything))]
    add x30 -> x0, other arithmetic: 6.58 us -> none  [the longest x15 6.36 us: combine_partial(): numer_a * factor_a[..., None] + numer_b * factor_b[..., None]]
  transfers between devices with their start and end apart: 3 -> 0, of which waited for: 3 -> 0; matrix products, arithmetic and copies ran while one was open for 0% -> 0% of each run, Pallas kernels for 0% -> 0%
where the time goes in v1:
time: 52.6 us; the launch traced here: 52.4 us
  Pallas kernels  51.1 us (97%)
  local copies, waits for them, and re-layouts  1.28 us (2%)
    pallas_call x1, Pallas kernels, fused(): pl.pallas_call(functools.partial(layer_kernel, n, feats * n), out_shape=j...  51.1 us
    unnamed x1, local copies, waits for them, and re-layouts  1.28 us

profile of v1, /device:TPU:0, one launch (start us, length us, event | category | flops | bytes accessed | tf_op | source)
XLA Modules:
  0.0 52.4 jit_solution(3128793688679630018)
XLA Ops:
  0.0 51.1 %shard_map.127 = bf16[8,256]{1,0:T(8,128)(2,1)} custom-call(bf16[8,256]{1,0:T(8,128)(2,1)} %tok_ref.1, f32[1,256]{1,0:T(1,128)} %bitcast.7, f32[8]{0:T(128)} %lam_ref.1, f32[1,256]{1,0:T(1,128)} %bitcast.8, f32[1,256]{1,0:T(1,128)} %bitcast.9, f32[1,128]{1,0:T(1,128)} %constant.4.clone.cos_ref, f32[1,128]{1,0:T(1,128)} %constant.5.clone.sin_ref, ...), custom_call_target="tpu_custom_call" | custom-call | tf_op jit(solution)/shard_map/pallas_call | solution.py:401
  51.1 1.3 %copy.15 = bf16[8,256]{1,0:T(8,128)(2,1)} copy(bf16[8,256]{1,0:T(8,128)(2,1)} %shard_map.127) | data formatting | bytes 8192
